TPU v7x, 32 devices: a whole 2x2x4 slice. The times are simulated.
32 devices in a mesh: grp: 2 (over y), tp: 4 (over z), dp: 4 (over x, core).
Axes of the slice: x: 2, y: 2, z: 4, core: 2. Of those that a mesh axis runs over, the one named last changes fastest.
Arguments:
- tokens: bfloat16 [512, 4096], P('grp', 'dp'), parts along dimension 0, may hold values from -40 to 40
- sequence_lengths: int32 [512], P(('grp', 'dp')), parts along dimension 0, may hold values from 1 to 4096, 262144 in all
- recurrent_state: float32 [2, 512, 128, 128], P(None, ('grp', 'dp'), 'tp'), parts along dimension 1, may hold values from -1.8 to 1.8
- norm_weight: float32 [2, 4096], P(None, 'dp'), may hold values from 0.1 to 1.9
- input_weight: bfloat16 [2, 4096, 2048], P(None, 'dp', 'tp'), may hold values from -0.09375 to 0.09375
- gate_weight: bfloat16 [2, 4096, 2048], P(None, 'dp', 'tp'), may hold values from -0.09375 to 0.09375
- output_weight: bfloat16 [2, 2048, 4096], P(None, 'tp', 'dp'), may hold values from -0.125 to 0.125
- negated_real_rate: float32 [2, 8192], P(None, 'tp'), may hold values from 0.005 to 1
- frequency: float32 [2, 8192], P(None, 'tp'), may hold values from -4 to 4
- discrete_step: float32 [2, 128], P(None, 'tp'), may hold values from 0.02 to 0.5
- group_input_matrix: float32 [2, 128, 16, 128], P(None, 'tp'), may hold values from -1.5 to 1.5
- group_output_matrix: float32 [2, 128, 16, 128], P(None, 'tp'), may hold values from -0.5 to 0.5
- feedthrough_weight: float32 [2, 2048], P(None, 'tp'), may hold values from -3 to 3
- extra_log_decay: float32 [2, 128, 4096], P(None, 'tp'), may hold values from -0.7 to 0
Outputs:
- tokens_out: bfloat16 [512, 4096], P('grp', 'dp'), parts along dimension 0
- state_out: float32 [2, 512, 128, 128], P(None, ('grp', 'dp'), 'tp'), parts along dimension 1
There are 2 independent parts, one for each index of `grp`. A program takes and returns all parts, laid end to end along the dimension named above; an argument that names none is the same for every part. Nothing has to cross between parts.
Inputs may be any that keep to these rules, and one draw needn't show every extreme that they name: The newest token of a sequence stands at position sequence_lengths - 1.
All inputs are finite; a program needn't handle non-finite values. No bound on the sum of `sequence_lengths` on one device may be relied on, other than what follows from the above.
Results may differ from a plain program's by a relative error of at most 0.009.
Values may be sent and summed in bfloat16 or wider, within the bound.
A program may use at most 64 MiB of HBM per device.

v0:
```python
import jax
import jax.numpy as jnp
from jax import lax
from jax.sharding import PartitionSpec as P

D = 4096
STACKED_LAYERS = 2
TOP_PRECISION = lax.Precision.HIGHEST
NORM_EPS = 1e-06


def transition(decay_factor, angular_frequency, step_width):
    log_mag = -decay_factor * step_width[:, None]
    turn = angular_frequency * step_width[:, None]
    magnitude = jnp.exp(log_mag)
    discrete_real = magnitude * jnp.cos(turn)
    discrete_imaginary = magnitude * jnp.sin(turn)
    half_sine = jnp.sin(0.5 * turn)
    numer_re = jnp.expm1(log_mag) * jnp.cos(turn) - 2.0 * half_sine * half_sine
    denom = decay_factor * decay_factor + angular_frequency * angular_frequency
    drive_re = (-numer_re * decay_factor + discrete_imaginary * angular_frequency) / denom
    drive_im = (-discrete_imaginary * decay_factor - numer_re * angular_frequency) / denom
    return (discrete_real, discrete_imaginary, drive_re, drive_im)


def state_space_update(
    input_groups,
    layer_state,
    extra_decay_factor,
    decay_factor,
    angular_frequency,
    step_width,
    input_matrix,
    readout_matrix,
):
    half_width = input_matrix.shape[-1] // 2
    decay_factor = decay_factor.reshape(-1, half_width)
    angular_frequency = angular_frequency.reshape(-1, half_width)
    discrete_real, discrete_imaginary, drive_re, drive_im = transition(
        decay_factor, angular_frequency, step_width
    )
    input_real = input_matrix[..., :half_width]
    input_imaginary = input_matrix[..., half_width:]
    driven_input_real = jnp.einsum(
        "tkl,klf->tkf", input_groups, input_real, precision=TOP_PRECISION
    )
    driven_input_imaginary = jnp.einsum(
        "tkl,klf->tkf", input_groups, input_imaginary, precision=TOP_PRECISION
    )
    state_re = layer_state[..., :half_width]
    state_im = layer_state[..., half_width:]
    carried_real = extra_decay_factor[..., None] * discrete_real[None]
    carried_imaginary = extra_decay_factor[..., None] * discrete_imaginary[None]
    updated_real = (
        carried_real * state_re
        - carried_imaginary * state_im
        + drive_re[None] * driven_input_real
        - drive_im[None] * driven_input_imaginary
    )
    updated_imaginary = (
        carried_real * state_im
        + carried_imaginary * state_re
        + drive_re[None] * driven_input_imaginary
        + drive_im[None] * driven_input_real
    )
    readout_rows = jnp.einsum(
        "hzk,dhk->dhz", readout_matrix[..., :half_width], updated_real, precision=TOP_PRECISION
    ) - jnp.einsum(
        "hzk,dhk->dhz", readout_matrix[..., half_width:], updated_imaginary, precision=TOP_PRECISION
    )
    return (readout_rows, jnp.concatenate([updated_real, updated_imaginary], axis=-1))


def single_layer(
    hidden_rows,
    sequence_lengths,
    layer_state,
    norm_scale_rows,
    input_matrix_weight,
    gate_matrix,
    output_matrix_weight,
    decay_factor,
    angular_frequency,
    step_width,
    input_matrix,
    readout_matrix,
    feedthrough_rows,
    extra_decay_rows,
):
    x_float = hidden_rows.astype(jnp.float32)
    square_sums = jnp.sum(x_float * x_float, axis=1)
    scaled_in = (x_float * norm_scale_rows[None, :]).astype(jnp.bfloat16)
    input_part = jnp.dot(scaled_in, input_matrix_weight, preferred_element_type=jnp.float32)
    gate_part = jnp.dot(scaled_in, gate_matrix, preferred_element_type=jnp.float32)
    local_rows = sequence_lengths.shape[0]
    input_sum, gate_sum, mine_squares = (
        lax.psum_scatter(input_part, "dp", scatter_dimension=0, tiled=True),
        lax.psum_scatter(gate_part, "dp", scatter_dimension=0, tiled=True),
        lax.psum_scatter(square_sums, "dp", scatter_dimension=0, tiled=True),
    )
    scale = lax.rsqrt(mine_squares / D + NORM_EPS)[:, None]
    u_vals = (input_sum * scale).astype(jnp.bfloat16)
    gate_vals = (gate_sum * scale).astype(jnp.bfloat16)
    group_count = layer_state.shape[1]
    input_float = u_vals.astype(jnp.float32)
    token_positions = sequence_lengths - 1
    extra_decay_factor = jnp.exp(jnp.take(extra_decay_rows, token_positions, axis=1).T)
    readout_rows, updated_state = state_space_update(
        input_float.reshape(local_rows, group_count, -1),
        layer_state,
        extra_decay_factor,
        decay_factor,
        angular_frequency,
        step_width,
        input_matrix,
        readout_matrix,
    )
    y_vals = jax.nn.gelu(
        readout_rows.reshape(local_rows, -1) + feedthrough_rows[None, :] * input_float
    )
    mixed = (y_vals * jax.nn.sigmoid(gate_vals.astype(jnp.float32))).astype(jnp.bfloat16)
    branch_terms = jnp.dot(
        lax.all_gather(mixed, "dp", axis=0, tiled=True),
        output_matrix_weight,
        preferred_element_type=jnp.float32,
    )
    branch = lax.psum(branch_terms, "tp").astype(jnp.bfloat16)
    x_next = (x_float + branch.astype(jnp.float32)).astype(jnp.bfloat16)
    return (x_next, updated_state)


def on_device(
    tokens,
    sequence_lengths,
    recurrent_state,
    norm_weight,
    input_weight,
    gate_weight,
    output_weight,
    negated_real_rate,
    frequency,
    discrete_step,
    group_input_matrix,
    group_output_matrix,
    feedthrough_weight,
    extra_log_decay,
):
    hidden_rows = tokens
    states = []
    for index_of_layer in range(STACKED_LAYERS):
        hidden_rows, updated_state = single_layer(
            hidden_rows,
            sequence_lengths,
            recurrent_state[index_of_layer],
            norm_weight[index_of_layer],
            input_weight[index_of_layer],
            gate_weight[index_of_layer],
            output_weight[index_of_layer],
            negated_real_rate[index_of_layer],
            frequency[index_of_layer],
            discrete_step[index_of_layer],
            group_input_matrix[index_of_layer],
            group_output_matrix[index_of_layer],
            feedthrough_weight[index_of_layer],
            extra_log_decay[index_of_layer],
        )
        states.append(updated_state)
    return (hidden_rows, jnp.stack(states, axis=0))


def solution(mesh):
    in_specs = (
        P("grp", "dp"),
        P(("grp", "dp")),
        P(None, ("grp", "dp"), "tp", None),
        P(None, "dp"),
        P(None, "dp", "tp"),
        P(None, "dp", "tp"),
        P(None, "tp", "dp"),
        P(None, "tp"),
        P(None, "tp"),
        P(None, "tp"),
        P(None, "tp", None, None),
        P(None, "tp", None, None),
        P(None, "tp"),
        P(None, "tp", None),
    )
    out_specs = (P("grp", "dp"), P(None, ("grp", "dp"), "tp", None))
    return jax.shard_map(
        on_device, mesh=mesh, in_specs=in_specs, out_specs=out_specs, check_vma=False
    )
```

profile of v0, /device:TPU:0, one launch (start us, length us, event | category | flops | bytes accessed | tf_op | source)
XLA Modules:
  0.0 220.6 jit_solution(5358436251447161086)
XLA Ops:
  8.0 2.6 %fusion.28 = f32[256,512]{1,0:T(8,128)} fusion(bf16[2,1024,512]{2,1,0:T(8,128)(2,1)} %param.20, bf16[256,1024]{1,0:T(8,128)(2,1)} %param.16, f32[1024]{0:T(1024)S(1)} %bitcast.103), kind=kOutput, calls=%fused_computation.51 | convolution fusion | flops 269221888 | bytes 2101248 | tf_op jit(solution)/shard_map/dot_general | solution.py:93
  10.8 2.6 %fusion.26 = f32[256,512]{1,0:T(8,128)} fusion(bf16[2,1024,512]{2,1,0:T(8,128)(2,1)} %param.21, bf16[256,1024]{1,0:T(8,128)(2,1)S(1)} %copy-done.3, f32[1024]{0:T(1024)S(1)} %bitcast.104), kind=kOutput, calls=%fused_computation.49 | convolution fusion | flops 269221888 | bytes 2101248 | tf_op jit(solution)/shard_map/dot_general | solution.py:94
  13.6 8.5 %all-reduce = f32[256]{0:T(256)S(1)} all-reduce(f32[256]{0:T(256)S(1)} %fusion.13), channel_id=3, replica_groups=mesh['grp'=2,'tp'=4,'dp'=4] {'dp'}, use_global_device_ids=true, to_apply=%region_2.4.clone | all-reduce | flops 256 | bytes 2048
  25.8 1.9 copy.51
  28.3 2.3 %gather_fusion = f32[64,32]{1,0:T(8,128)S(1)} fusion(f32[32,4096]{0,1:T(8,128)} %bitcast.92, s32[1024]{0:T(1024)S(1)} %pad_clamp_fusion), kind=kCustom, calls=%fused_computation.clone | custom fusion | bytes 16640 | tf_op jit(solution)/shard_map/jit(_take)/gather | solution.py:107
  30.7 1.7 fusion.83
  33.8 2.5 %copy_bitcast_fusion = (f32[64,32,128]{2,0,1:T(8,128)}, f32[64,32,128]{2,0,1:T(8,128)}) fusion(f32[1,64,32,128]{3,2,1,0:T(8,128)S(1)} %get-tuple-element.21, f32[1,64,32,128]{3,2,1,0:T(8,128)S(1)} %get-tuple-element.22), kind=kLoop, calls=%fused_computation.39 | loop fusion | bytes 4194304 | tf_op jit(solution)/shard_map/squeeze | solution.py:154
  38.5 2.8 %fusion.5 = (f32[64,32,64]{2,0,1:T(8,128)S(1)}, f32[64,32,64]{2,0,1:T(8,128)S(1)}) fusion(f32[32,64,64]{2,1,0:T(8,128)S(1)} %fusion.50, f32[64,32,128]{2,0,1:T(8,128)} %get-tuple-element.46, f32[32,64]{1,0:T(8,128)S(1)} %get-tuple-element.36, f32[32,64]{1,0:T(8,128)S(1)} %get-tuple-element.35, f32[32,64]{1,0:T(8,128)S(1)} %get-tuple-element.34, ...), kind=kOutput, calls=%fused_computation.24 | convolution fusion | flops 27262976 | bytes 2990080 | tf_op jit(solution)/shard_map/tkl,klf->tkf/dot_general | solution.py:44
  41.3 1.7 fusion.48
  43.0 1.8 convolution_subtract_fusion.1
  45.0 14.7 %reduce-scatter.7.cloned.1.call-done = f32[64,512]{1,0:T(8,128)} async-done(((f32[256,512]{1,0:T(8,128)}), f32[64,512]{1,0:T(8,128)}) %reduce-scatter.7.cloned.1.call-update) | async-done | bytes 131088 | tf_op jit(solution)/shard_map/reduce_scatter | solution.py:98
  60.7 5.8 %all_gather.6 = bf16[256,512]{1,0:T(8,128)(2,1)S(1)} all-gather(bf16[64,512]{1,0:T(8,128)(2,1)S(1)} %fusion.62), channel_id=1, replica_groups=mesh['grp'=2,'tp'=4,'dp'=4] {'dp'}, dimensions={0}, use_global_device_ids=true | all-gather | bytes 327680 | tf_op jit(solution)/shard_map/all_gather | solution.py:123
  66.5 1.7 fusion.24
  68.1 44.3 %all-reduce.4 = bf16[256,1024]{1,0:T(8,128)(2,1)} all-reduce(f32[256,1024]{1,0:T(8,128)S(1)} %fusion.24), channel_id=1, replica_groups=mesh['grp'=2,'tp'=4,'dp'=4] {'tp'}, use_global_device_ids=true, to_apply=%region_4.0 | all-reduce | flops 262144 | bytes 1572864 | tf_op jit(solution)/shard_map/psum | solution.py:127
  113.9 2.7 %fusion.22 = f32[256,512]{1,0:T(8,128)} fusion(bf16[2,1024,512]{2,1,0:T(8,128)(2,1)} %param.20, bf16[256,1024]{1,0:T(8,128)(2,1)S(1)} %get-tuple-element.14, f32[1024]{0:T(1024)S(1)} %bitcast.101), kind=kOutput, calls=%fused_computation.45 | convolution fusion | flops 269221888 | bytes 2101248 | tf_op jit(solution)/shard_map/dot_general | solution.py:93
  117.1 6.2 %all-reduce.1 = f32[256]{0:T(256)S(1)} all-reduce(f32[256]{0:T(256)S(1)} %get-tuple-element.13), channel_id=6, replica_groups=mesh['grp'=2,'tp'=4,'dp'=4] {'dp'}, use_global_device_ids=true, to_apply=%region_7.9.clone | all-reduce | flops 256 | bytes 2048
  126.2 10.6 %reduce-scatter.9.cloned.1.call-done = f32[64,512]{1,0:T(8,128)} async-done(((f32[256,512]{1,0:T(8,128)}), f32[64,512]{1,0:T(8,128)}) %reduce-scatter.9.cloned.1.call-update) | async-done | bytes 131088 | tf_op jit(solution)/shard_map/reduce_scatter | solution.py:97
  140.8 2.5 %copy.50 = f32[2,64,32,128]{3,2,1,0:T(8,128)} copy(f32[2,64,32,128]{3,1,2,0:T(8,128)S(1)} %pad_maximum_fusion) | data formatting | bytes 4194304
  143.3 1.7 fusion.41
  145.0 1.8 convolution_subtract_fusion
  147.0 13.8 %reduce-scatter.11.cloned.1.call-done = f32[64,512]{1,0:T(8,128)} async-done(((f32[256,512]{1,0:T(8,128)}), f32[64,512]{1,0:T(8,128)}) %reduce-scatter.11.cloned.1.call-update) | async-done | bytes 131088 | tf_op jit(solution)/shard_map/reduce_scatter | solution.py:98
  161.9 5.8 %all_gather.7 = bf16[256,512]{1,0:T(8,128)(2,1)S(1)} all-gather(bf16[64,512]{1,0:T(8,128)(2,1)S(1)} %fusion.71), channel_id=1, replica_groups=mesh['grp'=2,'tp'=4,'dp'=4] {'dp'}, dimensions={0}, use_global_device_ids=true | all-gather | bytes 327680 | tf_op jit(solution)/shard_map/all_gather | solution.py:123
  168.1 43.9 %all-reduce.5 = bf16[256,1024]{1,0:T(8,128)(2,1)S(1)} all-reduce(f32[256,1024]{1,0:T(8,128)S(1)} %fusion.18), channel_id=1, replica_groups=mesh['grp'=2,'tp'=4,'dp'=4] {'tp'}, use_global_device_ids=true, to_apply=%region_9.11 | all-reduce | flops 262144 | bytes 1572864 | tf_op jit(solution)/shard_map/psum | solution.py:127
  212.0 2.0 fusion.17
  (86 shorter events, 19.9 us)
Async XLA Ops:
  7.2 3.6 %copy-start.3 = (bf16[256,1024]{1,0:T(8,128)(2,1)S(1)}, bf16[256,1024]{1,0:T(8,128)(2,1)}, u32[]{:S(2)}) copy-start(bf16[256,1024]{1,0:T(8,128)(2,1)} %param.16) | copy-start | bytes 1572868
  7.2 29.4 %reduce-scatter.5.cloned.1.call-start = ((), (), s32[]{:S(2)}) async-start(), calls=%async_computation.4 | async-start | bytes 655360 | tf_op jit(solution)/shard_map/reduce_scatter | solution.py:97
  10.6 11.5 %copy-start.16 = (s32[64]{0:T(128)S(1)}, s32[64]{0:T(128)}, u32[]{:S(2)}) copy-start(s32[64]{0:T(128)} %param.17) | copy-start | bytes 772
  10.6 11.5 %copy-start.14 = (f32[2,32]{1,0:T(2,128)S(1)}, f32[2,32]{1,0:T(2,128)}, u32[]{:S(2)}) copy-start(f32[2,32]{1,0:T(2,128)} %param.25) | copy-start | bytes 772
  10.6 11.5 %copy-start.13 = (f32[2,512]{1,0:T(2,128)S(1)}, f32[2,512]{1,0:T(2,128)}, u32[]{:S(2)}) copy-start(f32[2,512]{1,0:T(2,128)} %param.28) | copy-start | bytes 12292
  10.6 11.6 %copy-start.11 = (f32[2,2048]{1,0:T(2,128)S(1)}, f32[2,2048]{1,0:T(2,128)}, u32[]{:S(2)}) copy-start(f32[2,2048]{1,0:T(2,128)} %param.24) | copy-start | bytes 49156
  10.7 11.6 %copy-start.12 = (f32[2,2048]{1,0:T(2,128)S(1)}, f32[2,2048]{1,0:T(2,128)}, u32[]{:S(2)}) copy-start(f32[2,2048]{1,0:T(2,128)} %param.23) | copy-start | bytes 49156
  10.7 11.8 %copy-start.7 = (f32[2,32,16,128]{3,2,1,0:T(8,128)S(1)}, f32[2,32,16,128]{3,2,1,0:T(8,128)}, u32[]{:S(2)}) copy-start(f32[2,32,16,128]{3,2,1,0:T(8,128)} %param.26) | copy-start | bytes 1572868
  10.7 12.5 %copy-start.8 = (f32[2,32,16,128]{3,2,1,0:T(8,128)S(1)}, f32[2,32,16,128]{3,2,1,0:T(8,128)}, u32[]{:S(2)}) copy-start(f32[2,32,16,128]{3,2,1,0:T(8,128)} %param.27) | copy-start | bytes 1572868
  10.7 48.9 %reduce-scatter.7.cloned.1.call-start = ((), (), s32[]{:S(2)}) async-start(), calls=%async_computation.5 | async-start | bytes 655360 | tf_op jit(solution)/shard_map/reduce_scatter | solution.py:98
  13.4 9.9 %copy-start.4 = (f32[2,32,4096]{2,1,0:T(8,128)S(1)}, f32[2,32,4096]{2,1,0:T(8,128)}, u32[]{:S(2)}) copy-start(f32[2,32,4096]{2,1,0:T(8,128)} %param.29) | copy-start | bytes 3145732
  13.4 123.4 %reduce-scatter.9.cloned.1.call-start = ((), (), s32[]{:S(2)}) async-start(), calls=%async_computation.6 | async-start | bytes 655360 | tf_op jit(solution)/shard_map/reduce_scatter | solution.py:97
  30.7 1.8 copy-start.17
  41.3 18.3 %copy-start.9 = (f32[64,512]{1,0:T(8,128)S(1)}, f32[64,512]{1,0:T(8,128)}, u32[]{:S(2)}) copy-start(f32[64,512]{1,0:T(8,128)} %reduce-scatter.5.cloned.1.call-done) | copy-start | bytes 393220
  113.9 9.3 %copy-start.1 = (bf16[256,1024]{1,0:T(8,128)(2,1)}, bf16[256,1024]{1,0:T(8,128)(2,1)S(1)}, u32[]{:S(2)}) copy-start(bf16[256,1024]{1,0:T(8,128)(2,1)S(1)} %get-tuple-element.14) | copy-start | bytes 1572868
  116.6 44.2 %reduce-scatter.11.cloned.1.call-start = ((), (), s32[]{:S(2)}) async-start(), calls=%async_computation.7 | async-start | bytes 655360 | tf_op jit(solution)/shard_map/reduce_scatter | solution.py:98
  123.2 1.6 copy-start.15
  123.3 1.6 copy-start.2
  124.9 13.0 %copy-start.6 = (f32[32,16,128]{2,1,0:T(8,128)S(1)}, f32[32,16,128]{2,1,0:T(8,128)}, u32[]{:S(2)}) copy-start(f32[32,16,128]{2,1,0:T(8,128)} %get-tuple-element.27) | copy-start | bytes 786436
  124.9 13.8 %copy-start.5 = (f32[64,32,128]{2,0,1:T(8,128)S(1)}, f32[64,32,128]{2,0,1:T(8,128)}, u32[]{:S(2)}) copy-start(f32[64,32,128]{2,0,1:T(8,128)} %get-tuple-element.45) | copy-start | bytes 3145732
  143.3 17.5 %copy-start.10 = (f32[64,512]{1,0:T(8,128)S(1)}, f32[64,512]{1,0:T(8,128)}, u32[]{:S(2)}) copy-start(f32[64,512]{1,0:T(8,128)} %reduce-scatter.9.cloned.1.call-done) | copy-start | bytes 393220
  143.3 24.3 %copy-start = (bf16[2,512,1024]{2,1,0:T(8,128)(2,1)S(1)}, bf16[2,512,1024]{2,1,0:T(8,128)(2,1)}, u32[]{:S(2)}) copy-start(bf16[2,512,1024]{2,1,0:T(8,128)(2,1)} %param.22) | copy-start | bytes 6291460
Sparse Core Ops, SparseCore 0:
  11.0 24.3 reduce-scatter.4
  38.0 21.6 reduce-scatter.6
  116.7 20.0 reduce-scatter.8
  139.1 21.6 reduce-scatter.10
where the time goes:
time: 221 us
  blocking collectives  114 us (52%)
  waiting for transfers between devices  39.2 us (18%)
  matrix products  24.2 us (11%)
  local copies, waits for them, and re-layouts  18.5 us (8%)
  between operations  14.8 us (7%)
  other arithmetic  9.38 us (4%)
    psum x2, blocking collectives, single_layer(): branch = lax.psum(branch_terms, 'tp').astype(jnp.bfloat16)  88.2 us
    reduce_scatter x2, waiting for transfers between devices, single_layer(): lax.psum_scatter(gate_part, 'dp', scatter_dimension=0, tiled=True)  28.5 us
    unnamed x2, blocking collectives  14.7 us
    all_gather x2, blocking collectives, single_layer(): lax.all_gather(mixed, 'dp', axis=0, tiled=True)  11.6 us
    reduce_scatter x2, waiting for transfers between devices, single_layer(): lax.psum_scatter(input_part, 'dp', scatter_dimension=0, tiled=True)  10.6 us
    unnamed x40, local copies, waits for them, and re-layouts  8.03 us
    dot_general x2, matrix products, single_layer(): jnp.dot(scaled_in, input_matrix_weight, preferred_element_type=jnp.float32)  5.28 us
  transfers between devices with their start and end apart: 4, of which 3 were waited for; matrix products, arithmetic and copies ran while one was open for 17% of the time, Pallas kernels for 0%

commit v1 on v0

--- a/solution.py
+++ b/solution.py
@@ -120,7 +120,15 @@
     )
     mixed = (y_vals * jax.nn.sigmoid(gate_vals.astype(jnp.float32))).astype(jnp.bfloat16)
     branch_terms = jnp.dot(
-        lax.all_gather(mixed, "dp", axis=0, tiled=True),
+        jnp.concatenate(
+            jax.lax.all_to_all(
+                jnp.stack([mixed for _ in range(jax.lax.psum(1, axis_name="dp"))], 0),
+                axis_name="dp",
+                split_axis=0,
+                concat_axis=0,
+            ),
+            0,
+        ),
         output_matrix_weight,
         preferred_element_type=jnp.float32,
     )

time: 221 us -> 229 us (1.036)
  matrix products: 24.2 us -> 28.8 us
  starting transfers between devices: 0.16 us -> 4.21 us
  blocking collectives: 114 us -> 111 us
    all_gather x2 -> x0, blocking collectives: 11.6 us -> none  [single_layer(): lax.all_gather(mixed, 'dp', axis=0, tiled=True)]
    all_to_all x0 -> x1, blocking collectives: none -> 8.39 us  [single_layer(): jax.lax.all_to_all(jnp.stack([mixed for _ in range(jax.lax.psum(1, axis_n...]
    all_to_all x0 -> x1, starting transfers between devices: none -> 4.05 us  [single_layer(): jax.lax.all_to_all(jnp.stack([mixed for _ in range(jax.lax.psum(1, axis_n...]
    all_to_all x0 -> x1, waiting for transfers between devices: none -> 2.92 us  [single_layer(): jax.lax.all_to_all(jnp.stack([mixed for _ in range(jax.lax.psum(1, axis_n...]
    unnamed x40 -> x44, local copies, waits for them, and re-layouts: 8.03 us -> 5.74 us
  transfers between devices with their start and end apart: 4 -> 5, of which waited for: 3 -> 4; matrix products, arithmetic and copies ran while one was open for 17% -> 18% of each run, Pallas kernels for 0% -> 0%
where the time goes in v1:
time: 229 us; the launch traced here: 228 us
  blocking collectives  111 us (48%)
  waiting for transfers between devices  41.3 us (18%)
  matrix products  28.8 us (13%)
  local copies, waits for them, and re-layouts  18.5 us (8%)
  between operations  14.8 us (6%)
  other arithmetic  10 us (4%)
  starting transfers between devices  4.21 us (2%)
    psum x2, blocking collectives, single_layer(): branch = lax.psum(branch_terms, 'tp').astype(jnp.bfloat16)  87.8 us
    reduce_scatter x2, waiting for transfers between devices, single_layer(): lax.psum_scatter(gate_part, 'dp', scatter_dimension=0, tiled=True)  28.9 us
    unnamed x2, blocking collectives  14.6 us
    reduce_scatter x2, waiting for transfers between devices, single_layer(): lax.psum_scatter(input_part, 'dp', scatter_dimension=0, tiled=True)  9.49 us
    all_to_all x1, blocking collectives, single_layer(): jax.lax.all_to_all(jnp.stack([mixed for _ in range(jax.lax.psum(1, axis_n...  8.39 us
    dot_general x2, matrix products, state_space_update(): jnp.einsum('tkl,klf->tkf', input_groups, input_real, precision=TOP_PRECIS...  5.9 us
    unnamed x44, local copies, waits for them, and re-layouts  5.74 us
    dot_general x2, matrix products, single_layer(): jnp.dot(scaled_in, input_matrix_weight, preferred_element_type=jnp.float32)  5.3 us
  transfers between devices with their start and end apart: 5, of which 4 were waited for; matrix products, arithmetic and copies ran while one was open for 18% of the time, Pallas kernels for 0%

profile of v1, /device:TPU:0, one launch (start us, length us, event | category | flops | bytes accessed | tf_op | source)
XLA Modules:
  0.0 228.4 jit_solution(17391862203603881752)
XLA Ops:
  8.0 2.6 %fusion.28 = f32[256,512]{1,0:T(8,128)} fusion(bf16[2,1024,512]{2,1,0:T(8,128)(2,1)} %param.20, bf16[256,1024]{1,0:T(8,128)(2,1)} %param.16, f32[1024]{0:T(1024)S(1)} %bitcast.106), kind=kOutput, calls=%fused_computation.51 | convolution fusion | flops 269221888 | bytes 2101248 | tf_op jit(solution)/shard_map/dot_general | solution.py:93
  10.8 2.6 %fusion.26 = f32[256,512]{1,0:T(8,128)} fusion(bf16[2,1024,512]{2,1,0:T(8,128)(2,1)} %param.21, bf16[256,1024]{1,0:T(8,128)(2,1)S(1)} %copy-done.3, f32[1024]{0:T(1024)S(1)} %bitcast.107), kind=kOutput, calls=%fused_computation.49 | convolution fusion | flops 269221888 | bytes 2101248 | tf_op jit(solution)/shard_map/dot_general | solution.py:94
  13.6 8.5 %all-reduce = f32[256]{0:T(256)S(1)} all-reduce(f32[256]{0:T(256)S(1)} %fusion.13), channel_id=3, replica_groups=mesh['grp'=2,'tp'=4,'dp'=4] {'dp'}, use_global_device_ids=true, to_apply=%region_2.4.clone | all-reduce | flops 256 | bytes 2048
  25.3 1.9 copy.51
  27.8 2.2 gather_fusion
  30.1 1.7 fusion.83
  33.2 2.5 %copy_bitcast_fusion = (f32[64,32,128]{2,0,1:T(8,128)}, f32[64,32,128]{2,0,1:T(8,128)}) fusion(f32[1,64,32,128]{3,2,1,0:T(8,128)S(1)} %get-tuple-element.21, f32[1,64,32,128]{3,2,1,0:T(8,128)S(1)} %get-tuple-element.22), kind=kLoop, calls=%fused_computation.39 | loop fusion | bytes 4194304 | tf_op jit(solution)/shard_map/squeeze | solution.py:162
  37.9 2.9 %fusion.5 = (f32[64,32,64]{2,0,1:T(8,128)S(1)}, f32[64,32,64]{2,0,1:T(8,128)S(1)}) fusion(f32[32,64,64]{2,1,0:T(8,128)S(1)} %fusion.50, f32[64,32,128]{2,0,1:T(8,128)} %get-tuple-element.46, f32[32,64]{1,0:T(8,128)S(1)} %get-tuple-element.36, f32[32,64]{1,0:T(8,128)S(1)} %get-tuple-element.35, f32[32,64]{1,0:T(8,128)S(1)} %get-tuple-element.34, ...), kind=kOutput, calls=%fused_computation.24 | convolution fusion | flops 27262976 | bytes 2990080 | tf_op jit(solution)/shard_map/tkl,klf->tkf/dot_general | solution.py:44
  42.6 1.8 convolution_subtract_fusion.1
  44.5 15.1 %reduce-scatter.7.cloned.1.call-done = f32[64,512]{1,0:T(8,128)} async-done(((f32[256,512]{1,0:T(8,128)}), f32[64,512]{1,0:T(8,128)}) %reduce-scatter.7.cloned.1.call-update) | async-done | bytes 131088 | tf_op jit(solution)/shard_map/reduce_scatter | solution.py:98
  60.7 8.4 %all_to_all.10 = bf16[4,64,512]{2,1,0:T(8,128)(2,1)S(1)} all-to-all(bf16[4,64,512]{2,1,0:T(8,128)(2,1)S(1)} %stack.10), channel_id=1, replica_groups=mesh['grp'=2,'tp'=4,'dp'=4] {'dp'}, dimensions={0} | all-to-all | bytes 524288 | tf_op jit(solution)/shard_map/all_to_all | solution.py:124
  70.8 44.2 %all-reduce.4 = bf16[256,1024]{1,0:T(8,128)(2,1)} all-reduce(f32[256,1024]{1,0:T(8,128)S(1)} %fusion.24), channel_id=1, replica_groups=mesh['grp'=2,'tp'=4,'dp'=4] {'tp'}, use_global_device_ids=true, to_apply=%region_4.0 | all-reduce | flops 262144 | bytes 1572864 | tf_op jit(solution)/shard_map/psum | solution.py:135
  116.4 2.7 %fusion.22 = f32[256,512]{1,0:T(8,128)} fusion(bf16[2,1024,512]{2,1,0:T(8,128)(2,1)} %param.20, bf16[256,1024]{1,0:T(8,128)(2,1)S(1)} %get-tuple-element.14, f32[1024]{0:T(1024)S(1)} %bitcast.104), kind=kOutput, calls=%fused_computation.45 | convolution fusion | flops 269221888 | bytes 2101248 | tf_op jit(solution)/shard_map/dot_general | solution.py:93
  120.6 6.1 %all-reduce.1 = f32[256]{0:T(256)S(1)} all-reduce(f32[256]{0:T(256)S(1)} %get-tuple-element.13), channel_id=6, replica_groups=mesh['grp'=2,'tp'=4,'dp'=4] {'dp'}, use_global_device_ids=true, to_apply=%region_7.9.clone | all-reduce | flops 256 | bytes 2048
  126.7 2.7 %fusion.20 = f32[256,512]{1,0:T(8,128)} fusion(bf16[2,1024,512]{2,1,0:T(8,128)(2,1)} %param.21, bf16[256,1024]{1,0:T(8,128)(2,1)} %copy-done.2, f32[1024]{0:T(1024)S(1)} %bitcast.105), kind=kOutput, calls=%fused_computation.43 | convolution fusion | flops 269221888 | bytes 2101248 | tf_op jit(solution)/shard_map/dot_general | solution.py:94
  129.4 9.5 %reduce-scatter.9.cloned.1.call-done = f32[64,512]{1,0:T(8,128)} async-done(((f32[256,512]{1,0:T(8,128)}), f32[64,512]{1,0:T(8,128)}) %reduce-scatter.9.cloned.1.call-update) | async-done | bytes 131088 | tf_op jit(solution)/shard_map/reduce_scatter | solution.py:97
  140.8 3.0 %fusion.11 = (f32[64,32,64]{2,0,1:T(8,128)S(1)}, f32[64,32,64]{2,0,1:T(8,128)S(1)}) fusion(f32[32,64,64]{2,1,0:T(8,128)S(1)} %fusion.43, f32[64,32,128]{2,0,1:T(8,128)} %get-tuple-element.45, f32[32,64]{1,0:T(8,128)} %get-tuple-element.32, f32[32,64]{1,0:T(8,128)} %get-tuple-element.31, f32[32,64]{1,0:T(8,128)} %get-tuple-element.30, ...), kind=kOutput, calls=%fused_computation.30 | convolution fusion | flops 27262976 | bytes 2990080 | tf_op jit(solution)/shard_map/tkl,klf->tkf/dot_general | solution.py:44
  145.5 2.5 %convolution_subtract_fusion = f32[32,64,16]{1,2,0:T(8,128)} fusion(f32[32,64,16]{1,2,0:T(8,128)S(1)} %fusion.41, f32[64,32,64]{2,0,1:T(8,128)S(1)} %get-tuple-element.17, f32[32,16,128]{2,1,0:T(8,128)S(1)} %get-tuple-element.25), kind=kOutput, calls=%fused_computation.17 | convolution fusion | flops 25198592 | bytes 1048576 | tf_op jit(solution)/shard_map/hzk,dhk->dhz/dot_general | solution.py:68
  149.1 13.8 %reduce-scatter.11.cloned.1.call-done = f32[64,512]{1,0:T(8,128)} async-done(((f32[256,512]{1,0:T(8,128)}), f32[64,512]{1,0:T(8,128)}) %reduce-scatter.11.cloned.1.call-update) | async-done | bytes 131088 | tf_op jit(solution)/shard_map/reduce_scatter | solution.py:98
  164.7 4.1 %all-to-all-start.1 = ((bf16[4,64,512]{2,1,0:T(8,128)(2,1)}), bf16[4,64,512]{2,1,0:T(8,128)(2,1)}, u32[]{:S(2)}, u32[]{:S(2)}) async-start(bf16[4,64,512]{2,1,0:T(8,128)(2,1)} %stack.11), calls=%async_computation.5 | async-start | bytes 524288 | tf_op jit(solution)/shard_map/all_to_all | solution.py:124
  169.4 2.5 %copy.50 = f32[2,64,32,128]{3,2,1,0:T(8,128)} copy(f32[2,64,32,128]{3,1,2,0:T(8,128)S(1)} %pad_maximum_fusion) | data formatting | bytes 4194304
  171.9 2.9 %all-to-all-done.1 = bf16[4,64,512]{2,1,0:T(8,128)(2,1)} async-done(((bf16[4,64,512]{2,1,0:T(8,128)(2,1)}), bf16[4,64,512]{2,1,0:T(8,128)(2,1)}, u32[]{:S(2)}, u32[]{:S(2)}) %all-to-all-start.1) | async-done | bytes 262176 | tf_op jit(solution)/shard_map/all_to_all | solution.py:124
  176.2 43.6 %all-reduce.5 = bf16[256,1024]{1,0:T(8,128)(2,1)S(1)} all-reduce(f32[256,1024]{1,0:T(8,128)S(1)} %fusion.18), channel_id=1, replica_groups=mesh['grp'=2,'tp'=4,'dp'=4] {'tp'}, use_global_device_ids=true, to_apply=%region_9.11 | all-reduce | flops 262144 | bytes 1572864 | tf_op jit(solution)/shard_map/psum | solution.py:135
  219.8 2.0 fusion.17
  (93 shorter events, 23.8 us)
Async XLA Ops:
  7.2 3.6 %copy-start.3 = (bf16[256,1024]{1,0:T(8,128)(2,1)S(1)}, bf16[256,1024]{1,0:T(8,128)(2,1)}, u32[]{:S(2)}) copy-start(bf16[256,1024]{1,0:T(8,128)(2,1)} %param.16) | copy-start | bytes 1572868
  7.2 28.8 %reduce-scatter.5.cloned.1.call-start = ((), (), s32[]{:S(2)}) async-start(), calls=%async_computation.6 | async-start | bytes 655360 | tf_op jit(solution)/shard_map/reduce_scatter | solution.py:97
  10.6 11.5 %copy-start.18 = (s32[64]{0:T(128)S(1)}, s32[64]{0:T(128)}, u32[]{:S(2)}) copy-start(s32[64]{0:T(128)} %param.17) | copy-start | bytes 772
  10.6 11.5 %copy-start.17 = (f32[2,32]{1,0:T(2,128)S(1)}, f32[2,32]{1,0:T(2,128)}, u32[]{:S(2)}) copy-start(f32[2,32]{1,0:T(2,128)} %param.25) | copy-start | bytes 772
  10.6 11.5 %copy-start.14 = (f32[2,512]{1,0:T(2,128)S(1)}, f32[2,512]{1,0:T(2,128)}, u32[]{:S(2)}) copy-start(f32[2,512]{1,0:T(2,128)} %param.28) | copy-start | bytes 12292
  10.6 12.1 %copy-start.11 = (f32[2,2048]{1,0:T(2,128)S(1)}, f32[2,2048]{1,0:T(2,128)}, u32[]{:S(2)}) copy-start(f32[2,2048]{1,0:T(2,128)} %param.24) | copy-start | bytes 49156
  10.7 12.1 %copy-start.12 = (f32[2,2048]{1,0:T(2,128)S(1)}, f32[2,2048]{1,0:T(2,128)}, u32[]{:S(2)}) copy-start(f32[2,2048]{1,0:T(2,128)} %param.23) | copy-start | bytes 49156
  10.7 12.3 %copy-start.7 = (f32[2,32,16,128]{3,2,1,0:T(8,128)S(1)}, f32[2,32,16,128]{3,2,1,0:T(8,128)}, u32[]{:S(2)}) copy-start(f32[2,32,16,128]{3,2,1,0:T(8,128)} %param.26) | copy-start | bytes 1572868
  10.7 13.1 %copy-start.8 = (f32[2,32,16,128]{3,2,1,0:T(8,128)S(1)}, f32[2,32,16,128]{3,2,1,0:T(8,128)}, u32[]{:S(2)}) copy-start(f32[2,32,16,128]{3,2,1,0:T(8,128)} %param.27) | copy-start | bytes 1572868
  10.7 48.9 %reduce-scatter.7.cloned.1.call-start = ((), (), s32[]{:S(2)}) async-start(), calls=%async_computation.7 | async-start | bytes 655360 | tf_op jit(solution)/shard_map/reduce_scatter | solution.py:98
  13.3 11.2 %copy-start.4 = (f32[2,32,4096]{2,1,0:T(8,128)S(1)}, f32[2,32,4096]{2,1,0:T(8,128)}, u32[]{:S(2)}) copy-start(f32[2,32,4096]{2,1,0:T(8,128)} %param.29) | copy-start | bytes 3145732
  13.4 125.5 %reduce-scatter.9.cloned.1.call-start = ((), (), s32[]{:S(2)}) async-start(), calls=%async_computation.8 | async-start | bytes 655360 | tf_op jit(solution)/shard_map/reduce_scatter | solution.py:97
  33.2 3.9 %copy-start.6 = (f32[32,16,128]{2,1,0:T(8,128)S(1)}, f32[32,16,128]{2,1,0:T(8,128)}, u32[]{:S(2)}) copy-start(f32[32,16,128]{2,1,0:T(8,128)} %get-tuple-element.28) | copy-start | bytes 786436
  37.9 3.0 %copy-start = (f32[32,16,128]{2,1,0:T(8,128)S(1)}, f32[32,16,128]{2,1,0:T(8,128)}, u32[]{:S(2)}) copy-start(f32[32,16,128]{2,1,0:T(8,128)} %get-tuple-element.26) | copy-start | bytes 786436
  40.8 18.8 %copy-start.9 = (f32[64,512]{1,0:T(8,128)S(1)}, f32[64,512]{1,0:T(8,128)}, u32[]{:S(2)}) copy-start(f32[64,512]{1,0:T(8,128)} %reduce-scatter.5.cloned.1.call-done) | copy-start | bytes 393220
  116.4 3.0 %copy-start.2 = (bf16[256,1024]{1,0:T(8,128)(2,1)}, bf16[256,1024]{1,0:T(8,128)(2,1)S(1)}, u32[]{:S(2)}) copy-start(bf16[256,1024]{1,0:T(8,128)(2,1)S(1)} %get-tuple-element.14) | copy-start | bytes 1572868
  119.1 43.8 %reduce-scatter.11.cloned.1.call-start = ((), (), s32[]{:S(2)}) async-start(), calls=%async_computation.9 | async-start | bytes 655360 | tf_op jit(solution)/shard_map/reduce_scatter | solution.py:98
  120.6 19.4 %copy-start.5 = (f32[32,16,128]{2,1,0:T(8,128)S(1)}, f32[32,16,128]{2,1,0:T(8,128)}, u32[]{:S(2)}) copy-start(f32[32,16,128]{2,1,0:T(8,128)} %get-tuple-element.27) | copy-start | bytes 786436
  126.7 12.2 %copy-start.15 = (f32[64]{0:T(128)}, f32[64]{0:T(128)S(1)}, u32[]{:S(2)}) copy-start(f32[64]{0:T(128)S(1)} %fusion.81) | copy-start | bytes 772
  143.8 19.1 %copy-start.10 = (f32[64,512]{1,0:T(8,128)S(1)}, f32[64,512]{1,0:T(8,128)}, u32[]{:S(2)}) copy-start(f32[64,512]{1,0:T(8,128)} %reduce-scatter.9.cloned.1.call-done) | copy-start | bytes 393220
  143.8 19.1 %copy-start.13 = (f32[1,512]{1,0:T(1,128)S(1)}, f32[1,512]{1,0:T(1,128)}, u32[]{:S(2)}) copy-start(f32[1,512]{1,0:T(1,128)} %get-tuple-element.39) | copy-start | bytes 6148
  143.8 19.1 %copy-start.16 = (f32[64]{0:T(128)S(1)}, f32[64]{0:T(128)}, u32[]{:S(2)}) copy-start(f32[64]{0:T(128)} %copy-done.15) | copy-start | bytes 772
  164.7 10.1 %all-to-all-start.1 = ((bf16[4,64,512]{2,1,0:T(8,128)(2,1)}), bf16[4,64,512]{2,1,0:T(8,128)(2,1)}, u32[]{:S(2)}, u32[]{:S(2)}) async-start(bf16[4,64,512]{2,1,0:T(8,128)(2,1)} %stack.11), calls=%async_computation.5 | async-start | bytes 524288 | tf_op jit(solution)/shard_map/all_to_all | solution.py:124
  169.4 5.5 %copy-start.1 = (bf16[2,512,1024]{2,1,0:T(8,128)(2,1)S(1)}, bf16[2,512,1024]{2,1,0:T(8,128)(2,1)}, u32[]{:S(2)}) copy-start(bf16[2,512,1024]{2,1,0:T(8,128)(2,1)} %param.22) | copy-start | bytes 6291460
  (1 other events, 1.8 us)
Sparse Core Ops, SparseCore 0:
  11.0 24.3 reduce-scatter.4
  37.9 21.6 reduce-scatter.6
  119.2 19.5 reduce-scatter.8
  141.2 21.6 reduce-scatter.10
